TPU v7x, 32 devices: a whole 2x2x4 slice. The times are simulated.
32 devices in a mesh: fs: 8 (over z, y), tp: 4 (over x, core).
Axes of the slice: x: 2, y: 2, z: 4, core: 2. Of those that a mesh axis runs over, the one named last changes fastest.
Arguments:
- prompt_tokens: bfloat16 [768, 4096], P('tp'), may hold values from -6 to 6
- norm_gain: float32 [4096], P('fs'), may hold values from 0.1 to 1.9
- gate_trained: float32 [4096, 11264], P('fs', 'tp'), may hold values from -0.09375 to 0.09375
- up_trained: float32 [4096, 11264], P('fs', 'tp'), may hold values from -0.09375 to 0.09375
- down_trained: float32 [11264, 4096], P('fs', 'tp'), may hold values from -0.078125 to 0.078125
Outputs:
- gate_serving: bfloat16 [4096, 11264], P(None, 'fs')
- up_serving: bfloat16 [4096, 11264], P(None, 'fs')
- down_serving: bfloat16 [11264, 4096], P('fs')
- mixed: bfloat16 [768, 4096], P('tp', 'fs')
All inputs are finite; a program needn't handle non-finite values.
Results may differ from a plain program's by a relative error of at most 0.0082.
Values may be sent and summed in bfloat16 or wider, within the bound.
A program may use at most 128 MiB of HBM per device.

v0:
```python
import jax
import jax.numpy as jnp
from jax import lax
from jax.sharding import PartitionSpec as P


def on_device(prompt_tokens, norm_gain, gate_trained, up_trained, down_trained):
    fs_count = lax.axis_size("fs")
    gate_cast = (gate_trained * norm_gain[:, None]).astype(jnp.bfloat16)
    up_cast = (up_trained * norm_gain[:, None]).astype(jnp.bfloat16)
    down_cast = down_trained.astype(jnp.bfloat16)
    down_serving = lax.all_gather(down_cast, "tp", axis=1, tiled=True)
    gate_part, up_part = (
        lax.all_to_all(gate_cast, "tp", split_axis=0, concat_axis=1, tiled=True),
        lax.all_to_all(up_cast, "tp", split_axis=0, concat_axis=1, tiled=True),
    )
    gate_mid, up_mid = (
        lax.all_to_all(gate_part, "fs", split_axis=1, concat_axis=0, tiled=True),
        lax.all_to_all(up_part, "fs", split_axis=1, concat_axis=0, tiled=True),
    )
    share = gate_mid.shape[0] // fs_count
    width = gate_mid.shape[1]
    gate_blocks, up_blocks = (
        lax.all_gather(gate_mid.reshape(fs_count, share, width), "tp", axis=1, tiled=True),
        lax.all_gather(up_mid.reshape(fs_count, share, width), "tp", axis=1, tiled=True),
    )
    gate_serving = gate_blocks.reshape(-1, width)
    up_serving = up_blocks.reshape(-1, width)
    tokens = prompt_tokens.astype(jnp.float32)
    scale = lax.rsqrt(jnp.mean(tokens * tokens, axis=-1, keepdims=True) + 1e-06)
    normed = (tokens * scale).astype(jnp.bfloat16)
    contract = (((0,), (1,)), ((), ()))
    gate_cols = lax.dot_general(gate_serving, normed, contract, preferred_element_type=jnp.float32)
    up_cols = lax.dot_general(up_serving, normed, contract, preferred_element_type=jnp.float32)
    hidden_cols = (jax.nn.silu(gate_cols) * up_cols).astype(jnp.bfloat16)
    summed = lax.psum_scatter(
        lax.dot_general(
            down_serving, hidden_cols, (((0,), (0,)), ((), ())), preferred_element_type=jnp.float32
        ),
        "fs",
        scatter_dimension=0,
        tiled=True,
    )
    mixed = summed.T.astype(jnp.bfloat16)
    return (gate_serving, up_serving, down_serving, mixed)


def solution(mesh):
    return jax.shard_map(
        on_device,
        mesh=mesh,
        in_specs=(P("tp", None), P("fs"), P("fs", "tp"), P("fs", "tp"), P("fs", "tp")),
        out_specs=(P(None, "fs"), P(None, "fs"), P("fs", None), P("tp", "fs")),
        check_vma=False,
    )
```

profile of v0, /device:TPU:0, one launch (start us, length us, event | category | flops | bytes accessed | tf_op | source)
XLA Modules:
  0.0 524.6 jit_solution(6554279546055345411)
XLA Ops:
  7.2 0.0 all-gather.4.cloned.1.call-start
  7.2 5.5 %multiply_convert_fusion = (bf16[512,2816]{1,0:T(8,128)(2,1)S(1)}, bf16[512,2816]{1,0:T(8,128)(2,1)S(1)}) fusion(f32[512,2816]{1,0:T(8,128)} %param.8, f32[512]{0:T(512)} %param.6, f32[512,2816]{1,0:T(8,128)} %param.7), kind=kLoop, calls=%fused_computation | loop fusion | flops 5767168 | bytes 17303552 | tf_op jit(solution)/shard_map/convert_element_type | solution.py:10
  12.7 38.2 %all_to_all.64 = bf16[4,128,2816]{2,1,0:T(8,128)(2,1)} all-to-all(bf16[4,128,2816]{2,1,0:T(8,128)(2,1)S(1)} %bitcast.18), channel_id=1, replica_groups=mesh['fs'=8,'tp'=4] {'tp'}, dimensions={0} | all-to-all | bytes 5767168 | tf_op jit(solution)/shard_map/all_to_all | solution.py:14
  51.0 4.5 copy.9
  55.5 71.4 %all_to_all.65 = bf16[128,8,1408]{0,2,1:T(8,128)(2,1)} all-to-all(bf16[128,8,1408]{0,2,1:T(8,128)(2,1)} %bitcast.26), channel_id=1, replica_groups=mesh['fs'=8,'tp'=4] {'fs'}, dimensions={1} | all-to-all | bytes 5767168 | tf_op jit(solution)/shard_map/all_to_all | solution.py:18
  126.9 0.0 all-gather.4.cloned.1.call-update
  126.9 0.0 all-gather.6.cloned.1.call-start
  127.0 64.5 %all_to_all.66 = bf16[4,128,2816]{2,1,0:T(8,128)(2,1)} all-to-all(bf16[4,128,2816]{2,1,0:T(8,128)(2,1)S(1)} %bitcast.17), channel_id=1, replica_groups=mesh['fs'=8,'tp'=4] {'tp'}, dimensions={0} | all-to-all | bytes 5767168 | tf_op jit(solution)/shard_map/all_to_all | solution.py:15
  191.5 3.3 copy.11
  194.8 67.9 %all_to_all.67 = bf16[128,8,1408]{0,2,1:T(8,128)(2,1)} all-to-all(bf16[128,8,1408]{0,2,1:T(8,128)(2,1)S(1)} %bitcast.28), channel_id=1, replica_groups=mesh['fs'=8,'tp'=4] {'fs'}, dimensions={1} | all-to-all | bytes 5767168 | tf_op jit(solution)/shard_map/all_to_all | solution.py:19
  262.7 0.0 all-gather.6.cloned.1.call-update
  262.8 0.0 all-gather.8.cloned.1.call-start
  262.8 4.7 convert_element_type.26
  267.5 0.0 copy-start
  267.5 0.0 all-gather.8.cloned.1.call-update
  267.5 0.0 reduce-scatter.2.cloned.1.call-start
  267.6 1.6 copy-done
  269.1 0.4 fusion
  269.5 0.0 all-gather.4.cloned.1.call-done
  269.6 16.0 %copy.10 = bf16[8,512,1408]{2,1,0:T(8,128)(2,1)} copy(bf16[8,512,1408]{1,2,0:T(8,128)(2,1)} %all-gather.4.cloned.1.call-done) | data formatting | bytes 23068672 | tf_op jit(solution)/shard_map/all_gather | solution.py:24
  285.6 53.0 %all-gather.6.cloned.1.call-done = bf16[8,512,1408]{1,2,0:T(8,128)(2,1)} async-done(((bf16[8,128,1408]{1,2,0:T(8,128)(2,1)}), bf16[8,512,1408]{1,2,0:T(8,128)(2,1)}) %all-gather.6.cloned.1.call-update) | async-done | bytes 11534352 | tf_op jit(solution)/shard_map/all_gather | solution.py:25
  338.5 16.0 %copy.12 = bf16[8,512,1408]{2,1,0:T(8,128)(2,1)} copy(bf16[8,512,1408]{1,2,0:T(8,128)(2,1)} %all-gather.6.cloned.1.call-done) | data formatting | bytes 23068672 | tf_op jit(solution)/shard_map/all_gather | solution.py:25
  354.5 7.2 %fusion.3 = f32[1408,192]{0,1:T(8,128)S(1)} fusion(bf16[4096,1408]{1,0:T(8,128)(2,1)} %bitcast.19, bf16[192,4096]{1,0:T(8,128)(2,1)S(1)} %copy-done, f32[192]{0:T(256)S(1)} %add_rsqrt_fusion), kind=kOutput, calls=%fused_computation.9 | convolution fusion | flops 2216951808 | bytes 14189312 | tf_op jit(solution)/shard_map/dot_general | solution.py:33
  361.8 55.1 %all-gather.8.cloned.1.call-done = bf16[1408,4096]{1,0:T(8,128)(2,1)} async-done(((bf16[1408,1024]{1,0:T(8,128)(2,1)}), bf16[1408,4096]{1,0:T(8,128)(2,1)}) %all-gather.8.cloned.1.call-update) | async-done | bytes 11534352 | tf_op jit(solution)/shard_map/all_gather | solution.py:12
  416.8 14.4 %convolution_bitcast_fusion = f32[4096,192]{0,1:T(8,128)} fusion(bf16[1408,4096]{1,0:T(8,128)(2,1)} %all-gather.8.cloned.1.call-done, bf16[4096,1408]{1,0:T(8,128)(2,1)} %bitcast.21, f32[1408,192]{0,1:T(8,128)S(1)} %fusion.3, bf16[192,4096]{1,0:T(8,128)(2,1)S(1)} %copy-done, f32[192]{0:T(256)S(1)} %add_rsqrt_fusion), kind=kOutput, calls=%fused_computation.2 | convolution fusion | flops 4433166336 | bytes 28869376 | tf_op jit(solution)/shard_map/dot_general | solution.py:37
  431.3 0.0 reduce-scatter.2.cloned.1.call-update
  431.3 75.0 %reduce-scatter.2.cloned.1.call-done = f32[512,192]{0,1:T(8,128)} async-done(((f32[4096,192]{0,1:T(8,128)}), f32[512,192]{0,1:T(8,128)}) %reduce-scatter.2.cloned.1.call-update) | async-done | bytes 393232 | tf_op jit(solution)/shard_map/reduce_scatter | solution.py:36
  506.3 1.7 convert_bitcast_fusion
  508.0 10.1 %copy.14 = bf16[1408,4096]{1,0:T(8,128)(2,1)} copy(bf16[1408,4096]{1,0:T(8,128)(2,1)} %all-gather.8.cloned.1.call-done) | data formatting | bytes 23068672
  (1 shorter events, 0.0 us)
Async XLA Ops:
  7.2 262.4 %all-gather.4.cloned.1.call-start = ((), (), s32[]{:S(2)}) async-start(), calls=%async_computation.5 | async-start | bytes 14417920 | tf_op jit(solution)/shard_map/all_gather | solution.py:24
  126.9 211.6 %all-gather.6.cloned.1.call-start = ((), (), s32[]{:S(2)}) async-start(), calls=%async_computation.6 | async-start | bytes 14417920 | tf_op jit(solution)/shard_map/all_gather | solution.py:25
  262.8 154.1 %all-gather.8.cloned.1.call-start = ((), (), s32[]{:S(2)}) async-start(), calls=%async_computation.7 | async-start | bytes 14417920 | tf_op jit(solution)/shard_map/all_gather | solution.py:12
  267.5 1.6 copy-start
  267.5 238.8 %reduce-scatter.2.cloned.1.call-start = ((), (), s32[]{:S(2)}) async-start(), calls=%async_computation.8 | async-start | bytes 3538944 | tf_op jit(solution)/shard_map/reduce_scatter | solution.py:36
Sparse Core Ops, SparseCore 0:
  127.1 102.4 all-gather.3
  262.9 75.5 all-gather.5
  340.7 76.1 all-gather.7
  431.4 74.8 reduce-scatter.1
where the time goes:
time: 526 us; the launch traced here: 525 us
  blocking collectives  242 us (46%)
  waiting for transfers between devices  183 us (35%)
  local copies, waits for them, and re-layouts  51.5 us (10%)
  matrix products  21.7 us (4%)
  between operations  13.8 us (3%)
  other arithmetic  12.3 us (2%)
    reduce_scatter x1, waiting for transfers between devices, on_device(): lax.psum_scatter(lax.dot_general(down_serving, hidden_cols, (((0,), (0,))...  75 us
    all_to_all x1, blocking collectives, on_device(): lax.all_to_all(gate_part, 'fs', split_axis=1, concat_axis=0, tiled=True)  71.4 us
    all_to_all x1, blocking collectives, on_device(): lax.all_to_all(up_part, 'fs', split_axis=1, concat_axis=0, tiled=True)  67.9 us
    all_to_all x1, blocking collectives, on_device(): lax.all_to_all(up_cast, 'tp', split_axis=0, concat_axis=1, tiled=True)  64.5 us
    all_gather x1, waiting for transfers between devices, on_device(): down_serving = lax.all_gather(down_cast, 'tp', axis=1, tiled=True)  55.1 us
    all_gather x1, waiting for transfers between devices, on_device(): lax.all_gather(up_mid.reshape(fs_count, share, width), 'tp', axis=1, tile...  53 us
    all_to_all x1, blocking collectives, on_device(): lax.all_to_all(gate_cast, 'tp', split_axis=0, concat_axis=1, tiled=True)  38.2 us
    all_gather x1, local copies, waits for them, and re-layouts, on_device(): lax.all_gather(up_mid.reshape(fs_count, share, width), 'tp', axis=1, tile...  16 us
  transfers between devices with their start and end apart: 4, of which 3 were waited for; matrix products, arithmetic and copies ran while one was open for 9% of the time, Pallas kernels for 0%

commit v1 on v0

--- a/solution.py
+++ b/solution.py
@@ -2,6 +2,23 @@
 import jax.numpy as jnp
 from jax import lax
 from jax.sharding import PartitionSpec as P
+
+
+def laid_out(pieces, dim):
+    pieces = jnp.moveaxis(pieces, 0, dim)
+    shape = pieces.shape
+    return pieces.reshape(*shape[:dim], shape[dim] * shape[dim + 1], *shape[dim + 2 :])
+
+
+def collected_by_bits(x, axis):
+    size, position = (lax.axis_size(axis), lax.axis_index(axis))
+    blocks, apart = (x[None], 1)
+    while apart < size:
+        other = lax.ppermute(blocks, axis, [(i, i ^ apart) for i in range(size)])
+        low = position & apart == 0
+        blocks = jnp.concatenate([jnp.where(low, blocks, other), jnp.where(low, other, blocks)])
+        apart *= 2
+    return blocks
 
 
 def on_device(prompt_tokens, norm_gain, gate_trained, up_trained, down_trained):
@@ -9,7 +26,7 @@
     gate_cast = (gate_trained * norm_gain[:, None]).astype(jnp.bfloat16)
     up_cast = (up_trained * norm_gain[:, None]).astype(jnp.bfloat16)
     down_cast = down_trained.astype(jnp.bfloat16)
-    down_serving = lax.all_gather(down_cast, "tp", axis=1, tiled=True)
+    down_serving = laid_out(collected_by_bits(down_cast, "tp"), 1)
     gate_part, up_part = (
         lax.all_to_all(gate_cast, "tp", split_axis=0, concat_axis=1, tiled=True),
         lax.all_to_all(up_cast, "tp", split_axis=0, concat_axis=1, tiled=True),

time: 526 us -> 606 us (1.15)
  waiting for transfers between devices: 183 us -> 256 us
  other arithmetic: 12.3 us -> 26 us
  local copies, waits for them, and re-layouts: 51.5 us -> 43.7 us
    ppermute x0 -> x2, waiting for transfers between devices: none -> 181 us  [collected_by_bits(): other = lax.ppermute(blocks, axis, [(i, i ^ apart) for i in range(size)])]
    all_gather x1 -> x0, waiting for transfers between devices: 55.1 us -> none  [on_device(): down_serving = lax.all_gather(down_cast, 'tp', axis=1, tiled=True)]
    all_gather x1, waiting for transfers between devices: 53 us -> 0.02 us  [on_device(): lax.all_gather(up_mid.reshape(fs_count, share, width), 'tp', axis=1, tile...]
    unnamed x3 -> x4, local copies, waits for them, and re-layouts: 11.7 us -> 0.15 us
    select_n x0 -> x2, other arithmetic: none -> 9.17 us  [collected_by_bits(): jnp.where(low, blocks, other)]
  transfers between devices with their start and end apart: 4 -> 5, of which waited for: 3 -> 3; matrix products, arithmetic and copies ran while one was open for 9% -> 8% of each run, Pallas kernels for 0% -> 0%
where the time goes in v1:
time: 606 us; the launch traced here: 605 us
  waiting for transfers between devices  256 us (42%)
  blocking collectives  242 us (40%)
  local copies, waits for them, and re-layouts  43.7 us (7%)
  other arithmetic  26 us (4%)
  matrix products  21.3 us (4%)
  between operations  13.8 us (2%)
    ppermute x2, waiting for transfers between devices, collected_by_bits(): other = lax.ppermute(blocks, axis, [(i, i ^ apart) for i in range(size)])  181 us
    reduce_scatter x1, waiting for transfers between devices, on_device(): lax.psum_scatter(lax.dot_general(down_serving, hidden_cols, (((0,), (0,))...  74.9 us
    all_to_all x1, blocking collectives, on_device(): lax.all_to_all(gate_part, 'fs', split_axis=1, concat_axis=0, tiled=True)  71.4 us
    all_to_all x1, blocking collectives, on_device(): lax.all_to_all(up_part, 'fs', split_axis=1, concat_axis=0, tiled=True)  67.9 us
    all_to_all x1, blocking collectives, on_device(): lax.all_to_all(up_cast, 'tp', split_axis=0, concat_axis=1, tiled=True)  64.5 us
    all_to_all x1, blocking collectives, on_device(): lax.all_to_all(gate_cast, 'tp', split_axis=0, concat_axis=1, tiled=True)  38.2 us
    all_gather x1, local copies, waits for them, and re-layouts, on_device(): lax.all_gather(gate_mid.reshape(fs_count, share, width), 'tp', axis=1, ti...  15.4 us
    all_gather x1, local copies, waits for them, and re-layouts, on_device(): lax.all_gather(up_mid.reshape(fs_count, share, width), 'tp', axis=1, tile...  15.3 us
  transfers between devices with their start and end apart: 5, of which 3 were waited for; matrix products, arithmetic and copies ran while one was open for 8% of the time, Pallas kernels for 0%

profile of v1, /device:TPU:0, one launch (start us, length us, event | category | flops | bytes accessed | tf_op | source)
XLA Modules:
  0.0 604.5 jit_solution(7218247534736713437)
XLA Ops:
  7.2 0.0 all-gather.3.cloned.1.call-start
  7.2 5.5 multiply_convert_fusion
  12.7 38.2 %all_to_all.64 = bf16[4,128,2816]{2,1,0:T(8,128)(2,1)} all-to-all(bf16[4,128,2816]{2,1,0:T(8,128)(2,1)S(1)} %bitcast.24), channel_id=1, replica_groups=mesh['fs'=8,'tp'=4] {'tp'}, dimensions={0} | all-to-all | bytes 5767168 | tf_op jit(solution)/shard_map/all_to_all | solution.py:31
  51.0 4.5 copy.11
  55.5 71.4 %all_to_all.65 = bf16[128,8,1408]{0,2,1:T(8,128)(2,1)} all-to-all(bf16[128,8,1408]{0,2,1:T(8,128)(2,1)} %bitcast.34), channel_id=1, replica_groups=mesh['fs'=8,'tp'=4] {'fs'}, dimensions={1} | all-to-all | bytes 5767168 | tf_op jit(solution)/shard_map/all_to_all | solution.py:35
  126.9 0.0 all-gather.3.cloned.1.call-update
  126.9 0.0 all-gather.5.cloned.1.call-start
  127.0 64.5 %all_to_all.66 = bf16[4,128,2816]{2,1,0:T(8,128)(2,1)} all-to-all(bf16[4,128,2816]{2,1,0:T(8,128)(2,1)S(1)} %bitcast.23), channel_id=1, replica_groups=mesh['fs'=8,'tp'=4] {'tp'}, dimensions={0} | all-to-all | bytes 5767168 | tf_op jit(solution)/shard_map/all_to_all | solution.py:32
  191.5 3.3 copy.13
  194.8 67.9 %all_to_all.67 = bf16[128,8,1408]{0,2,1:T(8,128)(2,1)} all-to-all(bf16[128,8,1408]{0,2,1:T(8,128)(2,1)S(1)} %bitcast.36), channel_id=1, replica_groups=mesh['fs'=8,'tp'=4] {'fs'}, dimensions={1} | all-to-all | bytes 5767168 | tf_op jit(solution)/shard_map/all_to_all | solution.py:36
  262.8 0.0 all-gather.5.cloned.1.call-update
  262.8 0.2 reduce-scatter.2.cloned.1.call-start
  263.0 3.1 convert_bitcast_fusion
  266.1 0.1 collective-permute-start
  266.2 5.5 collective-permute-done
  271.6 4.9 broadcast_select_fusion.3
  276.6 0.0 copy-start
  276.6 3.3 pad_maximum_fusion
  279.9 0.1 copy-done
  280.1 0.9 collective-permute-start.1
  281.0 1.8 fusion
  282.8 175.9 %collective-permute-done.1 = bf16[2,1408,1024]{2,1,0:T(8,128)(2,1)} collective-permute-done((bf16[2,1408,1024]{2,1,0:T(8,128)(2,1)}, bf16[2,1408,1024]{2,1,0:T(8,128)(2,1)}, u32[]{:S(2)}, u32[]{:S(2)}) %collective-permute-start.1) | collective-permute-done | bytes 5767200 | tf_op jit(solution)/shard_map/ppermute | solution.py:17
  458.8 4.2 broadcast_select_fusion.1
  463.0 1.4 maximum_bitcast_fusion
  464.4 5.0 copy.16
  469.4 0.0 copy-start.1
  469.4 0.0 all-gather.3.cloned.1.call-done
  469.4 15.4 %copy.12 = bf16[8,512,1408]{2,1,0:T(8,128)(2,1)} copy(bf16[8,512,1408]{1,2,0:T(8,128)(2,1)} %all-gather.3.cloned.1.call-done) | data formatting | bytes 23068672 | tf_op jit(solution)/shard_map/all_gather | solution.py:41
  484.8 0.0 copy-done.1
  484.8 6.9 %fusion.3 = f32[1408,192]{0,1:T(8,128)S(1)} fusion(bf16[4096,1408]{1,0:T(8,128)(2,1)} %bitcast.27, bf16[192,4096]{1,0:T(8,128)(2,1)S(1)} %copy-done.1, f32[192]{0:T(256)S(1)} %add_rsqrt_fusion), kind=kOutput, calls=%fused_computation.15 | convolution fusion | flops 2216951808 | bytes 14189312 | tf_op jit(solution)/shard_map/dot_general | solution.py:50
  491.7 0.0 all-gather.5.cloned.1.call-done
  491.7 15.3 %copy.14 = bf16[8,512,1408]{2,1,0:T(8,128)(2,1)} copy(bf16[8,512,1408]{1,2,0:T(8,128)(2,1)} %all-gather.5.cloned.1.call-done) | data formatting | bytes 23068672 | tf_op jit(solution)/shard_map/all_gather | solution.py:42
  507.0 14.3 %fusion.7 = f32[4096,192]{0,1:T(8,128)} fusion(bf16[1408,4096]{1,0:T(8,128)(2,1)} %bitcast.25, bf16[4096,1408]{1,0:T(8,128)(2,1)} %bitcast.29, f32[1408,192]{0,1:T(8,128)S(1)} %fusion.3, bf16[192,4096]{1,0:T(8,128)(2,1)S(1)} %copy-done.1, f32[192]{0:T(256)S(1)} %add_rsqrt_fusion), kind=kOutput, calls=%fused_computation.16 | convolution fusion | flops 4433166336 | bytes 28869376 | tf_op jit(solution)/shard_map/dot_general | solution.py:54
  521.3 0.0 reduce-scatter.2.cloned.1.call-update
  521.3 74.9 %reduce-scatter.2.cloned.1.call-done = f32[512,192]{0,1:T(8,128)} async-done(((f32[4096,192]{0,1:T(8,128)}), f32[512,192]{0,1:T(8,128)}) %reduce-scatter.2.cloned.1.call-update) | async-done | bytes 393232 | tf_op jit(solution)/shard_map/reduce_scatter | solution.py:53
  596.3 1.7 convert_bitcast_fusion.1
  (1 shorter events, 0.0 us)
Async XLA Ops:
  7.2 462.2 %all-gather.3.cloned.1.call-start = ((), (), s32[]{:S(2)}) async-start(), calls=%async_computation.5 | async-start | bytes 14417920 | tf_op jit(solution)/shard_map/all_gather | solution.py:41
  126.9 364.8 %all-gather.5.cloned.1.call-start = ((), (), s32[]{:S(2)}) async-start(), calls=%async_computation.6 | async-start | bytes 14417920 | tf_op jit(solution)/shard_map/all_gather | solution.py:42
  262.8 333.5 %reduce-scatter.2.cloned.1.call-start = ((), (), s32[]{:S(2)}) async-start(), calls=%async_computation.7 | async-start | bytes 3538944 | tf_op jit(solution)/shard_map/reduce_scatter | solution.py:53
  266.1 5.5 collective-permute-start
  276.6 3.5 copy-start
  280.1 178.7 %collective-permute-start.1 = (bf16[2,1408,1024]{2,1,0:T(8,128)(2,1)}, bf16[2,1408,1024]{2,1,0:T(8,128)(2,1)}, u32[]{:S(2)}, u32[]{:S(2)}) collective-permute-start(bf16[2,1408,1024]{2,1,0:T(8,128)(2,1)} %pad_maximum_fusion), channel_id=1, source_target_pairs={{0,2},{1,3},{2,0},{3,1},{4,6},{5,7},{6,4},{7,5},{8,10},{9,11},{10,... | collective-permute-start | bytes 17301512 | tf_op jit(solution)/shard_map/ppermute | solution.py:17
  469.4 15.4 %copy-start.1 = (bf16[192,4096]{1,0:T(8,128)(2,1)S(1)}, bf16[192,4096]{1,0:T(8,128)(2,1)}, u32[]{:S(2)}) copy-start(bf16[192,4096]{1,0:T(8,128)(2,1)} %param.5) | copy-start | bytes 4718596
Sparse Core Ops, SparseCore 0:
  127.1 102.4 all-gather.2
  262.9 127.5 all-gather.4
  521.5 74.7 reduce-scatter.1
